TPU v7x, 32 devices: a whole 2x2x4 slice. The times are simulated.
32 devices in a mesh: fs: 4 (over y, x), tp: 8 (over z, core).
Axes of the slice: x: 2, y: 2, z: 4, core: 2. Of those that a mesh axis runs over, the one named last changes fastest.
Arguments:
- inputs: bfloat16 [1536, 2048], P('fs'), may hold values from -6 to 6
- pre_act: bfloat16 [1536, 8192], P('fs', 'tp'), may hold values from -6 to 6
- cotangent: bfloat16 [1536, 2048], P('fs'), may hold values from -6 to 6
- up_weight: bfloat16 [2048, 8192], P('fs', 'tp'), may hold values from -0.125 to 0.125
- down_weight: bfloat16 [8192, 2048], P('tp', 'fs'), may hold values from -0.0625 to 0.0625
Outputs:
- input_grad: bfloat16 [1536, 2048], P('fs')
- up_grad: float32 [2048, 8192], P('fs', 'tp')
- down_grad: float32 [8192, 2048], P('tp', 'fs')
- up_norms: float32 [2048], P('fs')
- down_norms: float32 [8192], P('tp')
All inputs are finite; a program needn't handle non-finite values.
Results may differ from a plain program's by a relative error of at most 0.0051.
Values may be sent and summed in bfloat16 or wider, within the bound.
A program may use at most 64 MiB of HBM per device.

v0:
```python
import jax
import jax.numpy as jnp
from jax import lax
from jax.sharding import PartitionSpec as P


def contract_last(left, right):
    return lax.dot_general(
        left, right, (((1,), (1,)), ((), ())), preferred_element_type=jnp.float32
    )


def contract_first(left, right):
    return lax.dot_general(
        left, right, (((0,), (0,)), ((), ())), preferred_element_type=jnp.float32
    )


def local(inputs, pre_act, cotangent, up_weight, down_weight):
    active = jnp.maximum(pre_act.astype(jnp.float32), 0.0)
    squared = (active * active).astype(jnp.bfloat16)
    sq_grad = contract_last(cotangent, lax.all_gather(down_weight, "fs", axis=1, tiled=True))
    pre_grad = (2.0 * active * sq_grad).astype(jnp.bfloat16)
    partial_value = contract_last(pre_grad, lax.all_gather(up_weight, "fs", axis=0, tiled=True))
    input_grad = lax.psum(partial_value, "tp").astype(jnp.bfloat16)
    input_cols, cotan_cols = (
        lax.all_to_all(inputs, "fs", split_axis=1, concat_axis=0, tiled=True),
        lax.all_to_all(cotangent, "fs", split_axis=1, concat_axis=0, tiled=True),
    )
    all_pre_grad, all_squared = (
        lax.all_gather(pre_grad, "fs", axis=0, tiled=True),
        lax.all_gather(squared, "fs", axis=0, tiled=True),
    )
    up_grad = contract_first(input_cols, all_pre_grad)
    down_grad = contract_first(all_squared, cotan_cols)
    up_norms = lax.psum(jnp.sum(up_grad * up_grad, axis=1), "tp")
    down_norms = lax.psum(jnp.sum(down_grad * down_grad, axis=1), "fs")
    return (input_grad, up_grad, down_grad, up_norms, down_norms)


def solution(mesh):
    in_specs = (P("fs", None), P("fs", "tp"), P("fs", None), P("fs", "tp"), P("tp", "fs"))
    out_specs = (P("fs", None), P("fs", "tp"), P("tp", "fs"), P("fs"), P("tp"))
    return jax.shard_map(local, mesh=mesh, in_specs=in_specs, out_specs=out_specs, check_vma=False)
```

profile of v0, /device:TPU:0, one launch (start us, length us, event | category | flops | bytes accessed | tf_op | source)
XLA Modules:
  0.0 329.2 jit_solution(1895293256298894493)
XLA Ops:
  7.2 0.0 copy-start.2
  7.2 0.0 all-gather.5.cloned.1.call-start
  7.2 0.7 all-gather.5.cloned.1.call-update
  7.9 0.0 copy-start.1
  7.9 0.0 all-gather.11.cloned.1.call-start
  8.0 0.3 copy-done.2
  8.3 1.1 multiply_convert_fusion
  9.4 0.0 all-gather.11.cloned.1.call-update
  9.4 0.0 all-gather.7.cloned.1.call-start
  9.5 0.7 all-gather.7.cloned.1.call-update
  10.1 0.0 all-gather.9.cloned.1.call-start
  10.2 54.8 %all-gather.5.cloned.1.call-done = bf16[1024,2048]{1,0:T(8,128)(2,1)} async-done(((bf16[1024,512]{1,0:T(8,128)(2,1)}), bf16[1024,2048]{1,0:T(8,128)(2,1)}) %all-gather.5.cloned.1.call-update) | async-done | bytes 4194320 | tf_op jit(solution)/shard_map/all_gather | solution.py:22
  65.0 0.0 copy-done.1
  65.0 0.0 copy-start
  65.0 5.2 %multiply_convert_fusion.1 = bf16[384,1024]{1,0:T(8,128)(2,1)} fusion(bf16[384,1024]{1,0:T(8,128)(2,1)} %param.6, bf16[384,2048]{1,0:T(8,128)(2,1)S(1)} %copy-done.1, bf16[1024,2048]{1,0:T(8,128)(2,1)} %all-gather.5.cloned.1.call-done), kind=kOutput, calls=%fused_computation.4 | convolution fusion | flops 1612578816 | bytes 7340032 | tf_op jit(solution)/shard_map/dot_general | solution.py:8
  70.2 0.0 all-gather.9.cloned.1.call-update
  70.3 0.0 copy-done
  70.3 1.6 copy.14
  71.8 3.6 %all-to-all-start = ((bf16[384,4,512]{0,2,1:T(8,128)(2,1)}), bf16[384,4,512]{0,2,1:T(8,128)(2,1)S(1)}, u32[]{:S(2)}, u32[]{:S(2)}) async-start(bf16[384,4,512]{0,2,1:T(8,128)(2,1)} %bitcast), calls=%async_computation | async-start | bytes 3145728 | tf_op jit(solution)/shard_map/all_to_all | solution.py:27
  75.5 1.6 copy.16
  77.0 25.8 %all-to-all-done = bf16[384,4,512]{0,2,1:T(8,128)(2,1)S(1)} async-done(((bf16[384,4,512]{0,2,1:T(8,128)(2,1)}), bf16[384,4,512]{0,2,1:T(8,128)(2,1)S(1)}, u32[]{:S(2)}, u32[]{:S(2)}) %all-to-all-start) | async-done | bytes 1572896 | tf_op jit(solution)/shard_map/all_to_all | solution.py:27
  102.9 3.6 %all-to-all-start.1 = ((bf16[384,4,512]{0,2,1:T(8,128)(2,1)}), bf16[384,4,512]{0,2,1:T(8,128)(2,1)S(1)}, u32[]{:S(2)}, u32[]{:S(2)}) async-start(bf16[384,4,512]{0,2,1:T(8,128)(2,1)} %bitcast.4), calls=%async_computation.1 | async-start | bytes 3145728 | tf_op jit(solution)/shard_map/all_to_all | solution.py:28
  106.4 1.6 copy.15
  108.1 34.6 %all-to-all-done.1 = bf16[384,4,512]{0,2,1:T(8,128)(2,1)S(1)} async-done(((bf16[384,4,512]{0,2,1:T(8,128)(2,1)}), bf16[384,4,512]{0,2,1:T(8,128)(2,1)S(1)}, u32[]{:S(2)}, u32[]{:S(2)}) %all-to-all-start.1) | async-done | bytes 1572896 | tf_op jit(solution)/shard_map/all_to_all | solution.py:28
  142.7 1.6 copy.17
  144.3 0.0 all-gather.11.cloned.1.call-done
  144.3 4.2 %multiply_reduce_fusion = (f32[1024]{0:T(1024)S(1)}, f32[1024,512]{0,1:T(8,128)S(1)}) fusion(bf16[1536,1024]{1,0:T(8,128)(2,1)} %all-gather.11.cloned.1.call-done, bf16[1536,512]{1,0:T(8,128)(2,1)} %bitcast.19), kind=kOutput, calls=%fused_computation | convolution fusion | flops 1611660288 | bytes 6819840 | tf_op jit(solution)/shard_map/dot_general | solution.py:14
  148.5 1.8 copy.19
  150.3 9.8 %psum.23 = f32[1024]{0:T(1024)} all-reduce(f32[1024]{0:T(1024)S(1)} %get-tuple-element.24), channel_id=1, replica_groups=mesh['fs'=4,'tp'=8] {'fs'}, use_global_device_ids=true, to_apply=%region_4.0 | all-reduce | flops 1024 | bytes 8192 | tf_op jit(solution)/shard_map/psum | solution.py:37
  160.1 37.4 %all-gather.7.cloned.1.call-done = bf16[2048,1024]{1,0:T(8,128)(2,1)} async-done(((bf16[512,1024]{1,0:T(8,128)(2,1)}), bf16[2048,1024]{1,0:T(8,128)(2,1)}) %all-gather.7.cloned.1.call-update) | async-done | bytes 4194320 | tf_op jit(solution)/shard_map/all_gather | solution.py:24
  197.5 4.3 %fusion = f32[384,2048]{1,0:T(8,128)S(1)} fusion(bf16[384,1024]{1,0:T(8,128)(2,1)} %multiply_convert_fusion.1, bf16[2048,1024]{1,0:T(8,128)(2,1)} %all-gather.7.cloned.1.call-done), kind=kOutput, calls=%fused_computation.6 | convolution fusion | flops 1610612736 | bytes 8126464 | tf_op jit(solution)/shard_map/dot_general | solution.py:8
  201.7 41.9 %all-gather.9.cloned.1.call-done = bf16[1536,1024]{1,0:T(8,128)(2,1)} async-done(((bf16[384,1024]{1,0:T(8,128)(2,1)}), bf16[1536,1024]{1,0:T(8,128)(2,1)}) %all-gather.9.cloned.1.call-update) | async-done | bytes 3145744 | tf_op jit(solution)/shard_map/all_gather | solution.py:31
  243.6 5.5 %multiply_reduce_fusion.1 = (f32[512]{0:T(512)S(1)}, f32[512,1024]{0,1:T(8,128)}) fusion(bf16[1536,1024]{1,0:T(8,128)(2,1)} %all-gather.9.cloned.1.call-done, bf16[1536,512]{1,0:T(8,128)(2,1)} %bitcast.18), kind=kOutput, calls=%fused_computation.1 | convolution fusion | flops 1611660800 | bytes 6817792 | tf_op jit(solution)/shard_map/dot_general | solution.py:14
  249.1 2.9 copy.18
  252.0 70.7 %all-reduce.2 = (bf16[384,2048]{1,0:T(8,128)(2,1)}, f32[512]{0:T(512)}) all-reduce(f32[384,2048]{1,0:T(8,128)S(1)} %fusion, f32[512]{0:T(512)S(1)} %get-tuple-element.22), channel_id=1, replica_groups=mesh['fs'=4,'tp'=8] {'tp'}, use_global_device_ids=true, to_apply=%region_0.0 | all-reduce | flops 786944 | bytes 4722688 | tf_op jit(solution)/shard_map/psum | solution.py:25
Async XLA Ops:
  7.2 1.1 copy-start.2
  7.2 57.8 %all-gather.5.cloned.1.call-start = ((), (), s32[]{:S(2)}) async-start(), calls=%async_computation.2 | async-start | bytes 5242880 | tf_op jit(solution)/shard_map/all_gather | solution.py:22
  7.9 57.1 %copy-start.1 = (bf16[384,2048]{1,0:T(8,128)(2,1)S(1)}, bf16[384,2048]{1,0:T(8,128)(2,1)}, u32[]{:S(2)}) copy-start(bf16[384,2048]{1,0:T(8,128)(2,1)} %param.7) | copy-start | bytes 4718596
  7.9 136.4 %all-gather.11.cloned.1.call-start = ((), (), s32[]{:S(2)}) async-start(), calls=%async_computation.5 | async-start | bytes 3932160 | tf_op jit(solution)/shard_map/all_gather | solution.py:32
  9.4 188.1 %all-gather.7.cloned.1.call-start = ((), (), s32[]{:S(2)}) async-start(), calls=%async_computation.3 | async-start | bytes 5242880 | tf_op jit(solution)/shard_map/all_gather | solution.py:24
  10.1 233.5 %all-gather.9.cloned.1.call-start = ((), (), s32[]{:S(2)}) async-start(), calls=%async_computation.4 | async-start | bytes 3932160 | tf_op jit(solution)/shard_map/all_gather | solution.py:31
  65.0 5.3 %copy-start = (bf16[384,2048]{1,0:T(8,128)(2,1)S(1)}, bf16[384,2048]{1,0:T(8,128)(2,1)}, u32[]{:S(2)}) copy-start(bf16[384,2048]{1,0:T(8,128)(2,1)} %param.5) | copy-start | bytes 4718596
  71.8 31.0 %all-to-all-start = ((bf16[384,4,512]{0,2,1:T(8,128)(2,1)}), bf16[384,4,512]{0,2,1:T(8,128)(2,1)S(1)}, u32[]{:S(2)}, u32[]{:S(2)}) async-start(bf16[384,4,512]{0,2,1:T(8,128)(2,1)} %bitcast), calls=%async_computation | async-start | bytes 3145728 | tf_op jit(solution)/shard_map/all_to_all | solution.py:27
  102.9 39.8 %all-to-all-start.1 = ((bf16[384,4,512]{0,2,1:T(8,128)(2,1)}), bf16[384,4,512]{0,2,1:T(8,128)(2,1)S(1)}, u32[]{:S(2)}, u32[]{:S(2)}) async-start(bf16[384,4,512]{0,2,1:T(8,128)(2,1)} %bitcast.4), calls=%async_computation.1 | async-start | bytes 3145728 | tf_op jit(solution)/shard_map/all_to_all | solution.py:28
Sparse Core Ops, SparseCore 0:
  9.8 55.1 all-gather.4
  66.8 76.1 all-gather.10
  144.8 52.5 all-gather.6
  199.8 43.8 all-gather.8
where the time goes:
time: 330 us; the launch traced here: 329 us
  waiting for transfers between devices  196 us (59%)
  blocking collectives  80.5 us (24%)
  matrix products  19.2 us (6%)
  between operations  13.8 us (4%)
  local copies, waits for them, and re-layouts  11.4 us (3%)
  starting transfers between devices  7.33 us (2%)
    psum x1, blocking collectives, local(): input_grad = lax.psum(partial_value, 'tp').astype(jnp.bfloat16)  70.7 us
    all_gather x1, waiting for transfers between devices, local(): lax.all_gather(down_weight, 'fs', axis=1, tiled=True)  54.8 us
    all_gather x1, waiting for transfers between devices, local(): lax.all_gather(pre_grad, 'fs', axis=0, tiled=True)  41.9 us
    all_gather x1, waiting for transfers between devices, local(): lax.all_gather(up_weight, 'fs', axis=0, tiled=True)  37.4 us
    all_to_all x1, waiting for transfers between devices, local(): lax.all_to_all(cotangent, 'fs', split_axis=1, concat_axis=0, tiled=True)  34.6 us
    all_to_all x1, waiting for transfers between devices, local(): lax.all_to_all(inputs, 'fs', split_axis=1, concat_axis=0, tiled=True)  25.8 us
    psum x1, blocking collectives, local(): down_norms = lax.psum(jnp.sum(down_grad * down_grad, axis=1), 'fs')  9.78 us
    dot_general x2, matrix products, contract_first(): lax.dot_general(left, right, (((0,), (0,)), ((), ())), preferred_element_...  9.7 us
  transfers between devices with their start and end apart: 6, of which 5 were waited for; matrix products, arithmetic and copies ran while one was open for 7% of the time, Pallas kernels for 0%

commit v1 on v0

--- a/solution.py
+++ b/solution.py
@@ -2,6 +2,27 @@
 import jax.numpy as jnp
 from jax import lax
 from jax.sharding import PartitionSpec as P
+
+
+def joined_along(pieces, dim):
+    shape = list(pieces.shape[1:])
+    shape[dim] *= pieces.shape[0]
+    return jnp.moveaxis(pieces, 0, dim).reshape(shape)
+
+
+def grow_blocks(array, axis):
+    size, index = (lax.axis_size(axis), lax.axis_index(axis))
+    blocks, bit = (array[None], 1)
+    while bit < size:
+        other = lax.ppermute(blocks, axis, [(i, i ^ bit) for i in range(size)])
+        low = index & bit == 0
+        blocks = jnp.concatenate([jnp.where(low, blocks, other), jnp.where(low, other, blocks)])
+        bit *= 2
+    return blocks
+
+
+def collect(shard, axis, dim):
+    return joined_along(grow_blocks(shard, axis), dim)
 
 
 def contract_last(left, right):
@@ -21,7 +42,7 @@
     squared = (active * active).astype(jnp.bfloat16)
     sq_grad = contract_last(cotangent, lax.all_gather(down_weight, "fs", axis=1, tiled=True))
     pre_grad = (2.0 * active * sq_grad).astype(jnp.bfloat16)
-    partial_value = contract_last(pre_grad, lax.all_gather(up_weight, "fs", axis=0, tiled=True))
+    partial_value = contract_last(pre_grad, collect(up_weight, "fs", 0))
     input_grad = lax.psum(partial_value, "tp").astype(jnp.bfloat16)
     input_cols, cotan_cols = (
         lax.all_to_all(inputs, "fs", split_axis=1, concat_axis=0, tiled=True),

time: 330 us -> 315 us (0.955)
  waiting for transfers between devices: 196 us -> 165 us
  other arithmetic: 1.08 us -> 9.31 us
  starting transfers between devices: 7.33 us -> 14 us
    all_to_all x1, waiting for transfers between devices: 34.6 us -> 81.7 us  [local(): lax.all_to_all(cotangent, 'fs', split_axis=1, concat_axis=0, tiled=True)]
    all_gather x1, waiting for transfers between devices: 41.9 us -> 0.02 us  [local(): lax.all_gather(pre_grad, 'fs', axis=0, tiled=True)]
    all_gather x1 -> x0, waiting for transfers between devices: 37.4 us -> none  [local(): lax.all_gather(up_weight, 'fs', axis=0, tiled=True)]
    all_gather x1, waiting for transfers between devices: 54.8 us -> 62.5 us  [local(): lax.all_gather(down_weight, 'fs', axis=1, tiled=True)]
    all_to_all x1, waiting for transfers between devices: 25.8 us -> 19.7 us  [local(): lax.all_to_all(inputs, 'fs', split_axis=1, concat_axis=0, tiled=True)]
    ppermute x0 -> x2, starting transfers between devices: none -> 4.99 us  [grow_blocks(): other = lax.ppermute(blocks, axis, [(i, i ^ bit) for i in range(size)])]
    concatenate x0 -> x2, other arithmetic: none -> 3.86 us  [grow_blocks(): jnp.concatenate([jnp.where(low, blocks, other), jnp.where(low, other, blo...]
  transfers between devices with their start and end apart: 6 -> 7, of which waited for: 5 -> 3; matrix products, arithmetic and copies ran while one was open for 7% -> 11% of each run, Pallas kernels for 0% -> 0%
where the time goes in v1:
time: 315 us
  waiting for transfers between devices  165 us (52%)
  blocking collectives  79.9 us (25%)
  matrix products  19.1 us (6%)
  local copies, waits for them, and re-layouts  14 us (4%)
  starting transfers between devices  14 us (4%)
  between operations  13.9 us (4%)
  other arithmetic  9.31 us (3%)
    all_to_all x1, waiting for transfers between devices, local(): lax.all_to_all(cotangent, 'fs', split_axis=1, concat_axis=0, tiled=True)  81.7 us
    psum x1, blocking collectives, local(): input_grad = lax.psum(partial_value, 'tp').astype(jnp.bfloat16)  70.4 us
    all_gather x1, waiting for transfers between devices, local(): lax.all_gather(down_weight, 'fs', axis=1, tiled=True)  62.5 us
    all_to_all x1, waiting for transfers between devices, local(): lax.all_to_all(inputs, 'fs', split_axis=1, concat_axis=0, tiled=True)  19.7 us
    dot_general x2, matrix products, contract_first(): lax.dot_general(left, right, (((0,), (0,)), ((), ())), preferred_element_...  9.71 us
    psum x1, blocking collectives, local(): down_norms = lax.psum(jnp.sum(down_grad * down_grad, axis=1), 'fs')  9.55 us
    dot_general x2, matrix products, contract_last(): lax.dot_general(left, right, (((1,), (1,)), ((), ())), preferred_element_...  9.39 us
    unnamed x10, local copies, waits for them, and re-layouts  8.86 us
  transfers between devices with their start and end apart: 7, of which 3 were waited for; matrix products, arithmetic and copies ran while one was open for 11% of the time, Pallas kernels for 0%

profile of v1, /device:TPU:0, one launch (start us, length us, event | category | flops | bytes accessed | tf_op | source)
XLA Modules:
  0.0 314.8 jit_solution(9926232925607691505)
XLA Ops:
  7.2 0.0 copy-start.1
  7.2 0.0 all-gather.4.cloned.1.call-start
  7.2 0.7 all-gather.4.cloned.1.call-update
  7.9 0.0 all-gather.8.cloned.1.call-start
  8.0 2.2 multiply_convert_fusion
  10.2 0.0 all-gather.8.cloned.1.call-update
  10.2 0.0 all-gather.6.cloned.1.call-start
  10.2 0.0 copy-start
  10.3 3.0 collective-permute-start
  13.3 62.5 %all-gather.4.cloned.1.call-done = bf16[1024,2048]{1,0:T(8,128)(2,1)} async-done(((bf16[1024,512]{1,0:T(8,128)(2,1)}), bf16[1024,2048]{1,0:T(8,128)(2,1)}) %all-gather.4.cloned.1.call-update) | async-done | bytes 4194320 | tf_op jit(solution)/shard_map/all_gather | solution.py:43
  75.8 0.0 copy-done.1
  75.8 5.1 %multiply_convert_fusion.1 = bf16[384,1024]{1,0:T(8,128)(2,1)} fusion(bf16[384,1024]{1,0:T(8,128)(2,1)} %param.6, bf16[384,2048]{1,0:T(8,128)(2,1)S(1)} %copy-done.1, bf16[1024,2048]{1,0:T(8,128)(2,1)} %all-gather.4.cloned.1.call-done), kind=kOutput, calls=%fused_computation.8 | convolution fusion | flops 1612578816 | bytes 7340032 | tf_op jit(solution)/shard_map/dot_general | solution.py:29
  81.0 0.0 all-gather.6.cloned.1.call-update
  81.0 0.0 copy-done
  81.0 1.6 copy.14
  82.6 0.0 copy-start.2
  82.6 4.5 %all-to-all-start = ((bf16[384,4,512]{0,2,1:T(8,128)(2,1)}), bf16[384,4,512]{0,2,1:T(8,128)(2,1)}, u32[]{:S(2)}, u32[]{:S(2)}) async-start(bf16[384,4,512]{0,2,1:T(8,128)(2,1)} %bitcast.2), calls=%async_computation | async-start | bytes 3145728 | tf_op jit(solution)/shard_map/all_to_all | solution.py:48
  87.1 0.0 collective-permute-done
  87.1 0.0 copy-done.2
  87.1 1.4 broadcast_select_fusion.3
  88.5 1.5 pad_maximum_fusion.1
  90.0 2.0 collective-permute-start.1
  92.0 2.6 copy.16
  94.5 19.7 %all-to-all-done = bf16[384,4,512]{0,2,1:T(8,128)(2,1)} async-done(((bf16[384,4,512]{0,2,1:T(8,128)(2,1)}), bf16[384,4,512]{0,2,1:T(8,128)(2,1)}, u32[]{:S(2)}, u32[]{:S(2)}) %all-to-all-start) | async-done | bytes 1572896 | tf_op jit(solution)/shard_map/all_to_all | solution.py:48
  114.2 4.3 %all-to-all-start.1 = ((bf16[384,4,512]{0,2,1:T(8,128)(2,1)}), bf16[384,4,512]{0,2,1:T(8,128)(2,1)}, u32[]{:S(2)}, u32[]{:S(2)}) async-start(bf16[384,4,512]{0,2,1:T(8,128)(2,1)} %bitcast.20), calls=%async_computation.1 | async-start | bytes 3145728 | tf_op jit(solution)/shard_map/all_to_all | solution.py:49
  118.6 2.6 copy.15
  121.1 81.7 %all-to-all-done.1 = bf16[384,4,512]{0,2,1:T(8,128)(2,1)} async-done(((bf16[384,4,512]{0,2,1:T(8,128)(2,1)}), bf16[384,4,512]{0,2,1:T(8,128)(2,1)}, u32[]{:S(2)}, u32[]{:S(2)}) %all-to-all-start.1) | async-done | bytes 1572896 | tf_op jit(solution)/shard_map/all_to_all | solution.py:49
  202.8 2.6 copy.17
  205.4 0.0 collective-permute-done.1
  205.4 1.9 broadcast_select_fusion.1
  207.3 2.4 pad_maximum_fusion
  209.6 0.0 all-gather.8.cloned.1.call-done
  209.6 4.2 %multiply_reduce_fusion = (f32[1024]{0:T(1024)S(1)}, f32[1024,512]{0,1:T(8,128)S(1)}) fusion(bf16[1536,1024]{1,0:T(8,128)(2,1)} %all-gather.8.cloned.1.call-done, bf16[1536,512]{1,0:T(8,128)(2,1)} %bitcast.23), kind=kOutput, calls=%fused_computation.2 | convolution fusion | flops 1611660288 | bytes 6819840 | tf_op jit(solution)/shard_map/dot_general | solution.py:35
  213.8 1.8 copy.19
  215.6 9.6 %psum.23 = f32[1024]{0:T(1024)} all-reduce(f32[1024]{0:T(1024)S(1)} %get-tuple-element.28), channel_id=1, replica_groups=mesh['fs'=4,'tp'=8] {'fs'}, use_global_device_ids=true, to_apply=%region_4.5 | all-reduce | flops 1024 | bytes 8192 | tf_op jit(solution)/shard_map/psum | solution.py:58
  225.2 4.3 %fusion = f32[384,2048]{1,0:T(8,128)S(1)} fusion(bf16[384,1024]{1,0:T(8,128)(2,1)} %multiply_convert_fusion.1, bf16[2048,1024]{1,0:T(8,128)(2,1)} %bitcast.21), kind=kOutput, calls=%fused_computation.12 | convolution fusion | flops 1610612736 | bytes 8126464 | tf_op jit(solution)/shard_map/dot_general | solution.py:29
  229.4 0.0 all-gather.6.cloned.1.call-done
  229.5 5.5 %multiply_reduce_fusion.1 = (f32[512]{0:T(512)S(1)}, f32[512,1024]{0,1:T(8,128)}) fusion(bf16[1536,1024]{1,0:T(8,128)(2,1)} %all-gather.6.cloned.1.call-done, bf16[1536,512]{1,0:T(8,128)(2,1)} %bitcast.22), kind=kOutput, calls=%fused_computation.3 | convolution fusion | flops 1611660800 | bytes 6817792 | tf_op jit(solution)/shard_map/dot_general | solution.py:35
  235.0 2.9 copy.18
  237.9 70.4 %all-reduce.2 = (bf16[384,2048]{1,0:T(8,128)(2,1)}, f32[512]{0:T(512)}) all-reduce(f32[384,2048]{1,0:T(8,128)S(1)} %fusion, f32[512]{0:T(512)S(1)} %get-tuple-element.26), channel_id=1, replica_groups=mesh['fs'=4,'tp'=8] {'tp'}, use_global_device_ids=true, to_apply=%region_0.1 | all-reduce | flops 786944 | bytes 4722688 | tf_op jit(solution)/shard_map/psum | solution.py:46
Async XLA Ops:
  7.2 68.7 %copy-start.1 = (bf16[384,2048]{1,0:T(8,128)(2,1)S(1)}, bf16[384,2048]{1,0:T(8,128)(2,1)}, u32[]{:S(2)}) copy-start(bf16[384,2048]{1,0:T(8,128)(2,1)} %param.7) | copy-start | bytes 4718596
  7.2 68.7 %all-gather.4.cloned.1.call-start = ((), (), s32[]{:S(2)}) async-start(), calls=%async_computation.2 | async-start | bytes 5242880 | tf_op jit(solution)/shard_map/all_gather | solution.py:43
  7.9 201.7 %all-gather.8.cloned.1.call-start = ((), (), s32[]{:S(2)}) async-start(), calls=%async_computation.4 | async-start | bytes 3932160 | tf_op jit(solution)/shard_map/all_gather | solution.py:53
  10.2 219.3 %all-gather.6.cloned.1.call-start = ((), (), s32[]{:S(2)}) async-start(), calls=%async_computation.3 | async-start | bytes 3932160 | tf_op jit(solution)/shard_map/all_gather | solution.py:52
  10.2 70.8 %copy-start = (bf16[384,2048]{1,0:T(8,128)(2,1)S(1)}, bf16[384,2048]{1,0:T(8,128)(2,1)}, u32[]{:S(2)}) copy-start(bf16[384,2048]{1,0:T(8,128)(2,1)} %param.5) | copy-start | bytes 4718596
  10.3 76.9 %collective-permute-start = (bf16[1,512,1024]{2,1,0:T(8,128)(2,1)}, bf16[1,512,1024]{2,1,0:T(8,128)(2,1)}, u32[]{:S(2)}, u32[]{:S(2)}) collective-permute-start(bf16[1,512,1024]{2,1,0:T(8,128)(2,1)} %bitcast.24), channel_id=1, source_target_pairs={{0,8},{8,0},{16,24},{24,16},{1,9},{9,1},{17,25},{25,17},{2,10},{10... | collective-permute-start | bytes 3145736 | tf_op jit(solution)/shard_map/ppermute | solution.py:17
  82.6 4.6 %copy-start.2 = (bf16[512,1024]{1,0:T(8,128)(2,1)S(1)}, bf16[512,1024]{1,0:T(8,128)(2,1)}, u32[]{:S(2)}) copy-start(bf16[512,1024]{1,0:T(8,128)(2,1)} %param.8) | copy-start | bytes 3145732
  82.6 31.6 %all-to-all-start = ((bf16[384,4,512]{0,2,1:T(8,128)(2,1)}), bf16[384,4,512]{0,2,1:T(8,128)(2,1)}, u32[]{:S(2)}, u32[]{:S(2)}) async-start(bf16[384,4,512]{0,2,1:T(8,128)(2,1)} %bitcast.2), calls=%async_computation | async-start | bytes 3145728 | tf_op jit(solution)/shard_map/all_to_all | solution.py:48
  90.0 115.4 %collective-permute-start.1 = (bf16[2,512,1024]{2,1,0:T(8,128)(2,1)}, bf16[2,512,1024]{2,1,0:T(8,128)(2,1)}, u32[]{:S(2)}, u32[]{:S(2)}) collective-permute-start(bf16[2,512,1024]{2,1,0:T(8,128)(2,1)} %pad_maximum_fusion.1), channel_id=1, source_target_pairs={{0,16},{8,24},{16,0},{24,8},{1,17},{9,25},{17,1},{25,9},{2,18},{10... | collective-permute-start | bytes 6291464 | tf_op jit(solution)/shard_map/ppermute | solution.py:17
  114.2 88.6 %all-to-all-start.1 = ((bf16[384,4,512]{0,2,1:T(8,128)(2,1)}), bf16[384,4,512]{0,2,1:T(8,128)(2,1)}, u32[]{:S(2)}, u32[]{:S(2)}) async-start(bf16[384,4,512]{0,2,1:T(8,128)(2,1)} %bitcast.20), calls=%async_computation.1 | async-start | bytes 3145728 | tf_op jit(solution)/shard_map/all_to_all | solution.py:49
Sparse Core Ops, SparseCore 0:
  9.8 65.9 all-gather.3
  77.7 84.3 all-gather.7
  163.9 53.9 all-gather.5
